TPU v7x, 32 devices: a whole 2x2x4 slice. The times are simulated.
32 devices in a mesh: sp: 4 (over z), tp: 4 (over y, x), dp: 2 (over core).
Axes of the slice: x: 2, y: 2, z: 4, core: 2. Of those that a mesh axis runs over, the one named last changes fastest.
Arguments:
- latent: bfloat16 [8192, 2048], P(('dp', 'sp', 'tp')), parts along dimension 0, may hold values from -6 to 6
- cond: bfloat16 [4096], P('dp'), parts along dimension 0, may hold values from -6 to 6
- ctx_rows: bfloat16 [2048, 2048], P(('dp', 'sp')), parts along dimension 0, may hold values from -6 to 6
- ctx_cond: bfloat16 [2048], replicated, may hold values from -6 to 6
- mod_weight: bfloat16 [3, 2048, 2048], P(None, 'sp', 'tp'), may hold values from -0.125 to 0.125
- norm_gain: float32 [2048], replicated, may hold values from 0.1 to 1.9
- out_gain: float32 [2048], replicated, may hold values from 0.1 to 1.9
- w_query: bfloat16 [2048, 1024], replicated, may hold values from -16 to 16
- w_key: bfloat16 [2048, 256], replicated, may hold values from -1 to 1
- w_value: bfloat16 [2048, 256], replicated, may hold values from -0.125 to 0.125
- w_out: bfloat16 [1024, 2048], replicated, may hold values from -0.1875 to 0.1875
- sink: float32 [16], replicated, may hold values from 3 to 8
Outputs:
- updated: bfloat16 [8192, 2048], P(('dp', 'sp', 'tp')), parts along dimension 0
There are 2 independent parts, one for each index of `dp`. A program takes and returns all parts, laid end to end along the dimension named above; an argument that names none is the same for every part. Nothing has to cross between parts.
All inputs are finite; a program needn't handle non-finite values.
Results may differ from a plain program's by a relative error of at most 0.0053.
Values may be sent and summed in bfloat16 or wider, within the bound.
A program may use at most 128 MiB of HBM per device.

v0:
```python
import jax
import jax.numpy as jnp
from jax import lax
from jax.sharding import PartitionSpec as P

HEAD_DIM = 64
WINDOW = 128
SPAN = 128
GRID_W = 64


EPSILON = 1e-06
NEG_BIG = -1e30


def extended(cells, sides, width):
    for axis, dim in sides:
        count = lax.axis_size(axis)
        ends = count - 1
        head = lax.slice_in_dim(cells, 0, width, axis=dim)
        tail = lax.slice_in_dim(cells, cells.shape[dim] - width, cells.shape[dim], axis=dim)
        cells = jnp.concatenate(
            [
                lax.ppermute(tail, axis, [(i, (i + 1) % count) for i in range(ends)]),
                cells,
                lax.ppermute(head, axis, [((i + 1) % count, i) for i in range(ends)]),
            ],
            axis=dim,
        )
    return cells


def rope_angles(positions, head_width):
    freq_count = head_width // 4
    inverse = 10000.0 ** (-jnp.arange(freq_count, dtype=jnp.float32) / freq_count)
    grid_row = (positions // GRID_W).astype(jnp.float32)
    grid_col = (positions % GRID_W).astype(jnp.float32)
    angles = jnp.concatenate([grid_row[:, None] * inverse, grid_col[:, None] * inverse], axis=-1)
    return (jnp.cos(angles), jnp.sin(angles))


def rotate(values, cosine, sine_table):
    half_width = values.shape[-1] // 2
    floats = values.astype(jnp.float32)
    first = floats[..., :half_width]
    second = floats[..., half_width:]
    cos_b = cosine[:, None]
    sin_b = sine_table[:, None]
    return jnp.concatenate(
        [first * cos_b - second * sin_b, first * sin_b + second * cos_b], axis=-1
    ).astype(jnp.bfloat16)


def mod_norm(rows, gain, scale_vec, shift_vec):
    floats = rows.astype(jnp.float32)
    normed = floats * lax.rsqrt(jnp.mean(floats * floats, axis=-1, keepdims=True) + EPSILON) * gain
    return (normed * (1.0 + scale_vec) + shift_vec).astype(jnp.bfloat16)


def band_attention(
    query_rot,
    query_plain,
    key_padded,
    value_padded,
    key_ctx,
    value_ctx,
    sink_group,
    offset,
    seq_total,
):
    length_dev, groups, head_width = query_rot.shape
    blocks = length_dev // SPAN
    query_blocks = query_rot.reshape(blocks, SPAN, groups, head_width)
    plain_blocks = query_plain.reshape(blocks, SPAN, groups, head_width)
    key_split = key_padded.reshape(blocks + 2, SPAN, head_width)
    value_split = value_padded.reshape(blocks + 2, SPAN, head_width)
    key_band = jnp.concatenate([key_split[:-2], key_split[1:-1], key_split[2:]], axis=1)
    value_band = jnp.concatenate([value_split[:-2], value_split[1:-1], value_split[2:]], axis=1)
    factor = head_width ** (-0.5)
    local = (
        jnp.einsum("nigd,njd->ngij", query_blocks, key_band, preferred_element_type=jnp.float32)
        * factor
    )
    block_start = offset + jnp.arange(blocks, dtype=jnp.int32) * SPAN
    query_pos = block_start[:, None, None] + jnp.arange(SPAN, dtype=jnp.int32)[None, :, None]
    key_pos = (
        block_start[:, None, None] + jnp.arange(3 * SPAN, dtype=jnp.int32)[None, None, :] - SPAN
    )
    allowed = (jnp.abs(query_pos - key_pos) <= WINDOW) & (key_pos >= 0) & (key_pos < seq_total)
    local = jnp.where(allowed[:, None], local, NEG_BIG)
    context = (
        jnp.einsum("nigd,cd->ngic", plain_blocks, key_ctx, preferred_element_type=jnp.float32)
        * factor
    )
    sink_col = sink_group[None, :, None]
    row_max = jnp.maximum(jnp.maximum(jnp.max(local, axis=-1), jnp.max(context, axis=-1)), sink_col)
    exp_local = jnp.exp(local - row_max[..., None])
    exp_ctx = jnp.exp(context - row_max[..., None])
    exp_sink = jnp.exp(sink_col - row_max)
    denom = jnp.sum(exp_local, axis=-1) + jnp.sum(exp_ctx, axis=-1) + exp_sink
    weight_local = (exp_local / denom[..., None]).astype(jnp.bfloat16)
    weight_ctx = (exp_ctx / denom[..., None]).astype(jnp.bfloat16)
    mixed = jnp.einsum(
        "ngij,njd->nigd", weight_local, value_band, preferred_element_type=jnp.float32
    ) + jnp.einsum("ngic,cd->nigd", weight_ctx, value_ctx, preferred_element_type=jnp.float32)
    return mixed.astype(jnp.bfloat16).reshape(length_dev, groups * head_width)


def shards(
    latent,
    cond,
    ctx_rows,
    ctx_cond,
    mod_weight,
    norm_gain,
    out_gain,
    w_query,
    w_key,
    w_value,
    w_out,
    sink,
):
    sp_size = lax.axis_size("sp")
    tp_size = lax.axis_size("tp")
    sp_index = lax.axis_index("sp")
    tp_index = lax.axis_index("tp")
    row_piece = mod_weight.shape[1]
    head_width = HEAD_DIM
    kv_count = w_key.shape[1] // head_width
    group_size = w_query.shape[1] // w_key.shape[1]
    vectors = jax.nn.silu(jnp.stack([cond, ctx_cond]).astype(jnp.float32)).astype(jnp.bfloat16)
    own_rows = lax.dynamic_slice_in_dim(vectors, sp_index * row_piece, row_piece, 1)
    shift_part = jnp.dot(own_rows, mod_weight[0], preferred_element_type=jnp.float32)
    scale_part = jnp.dot(own_rows, mod_weight[1], preferred_element_type=jnp.float32)
    gate_part = jnp.dot(own_rows[:1], mod_weight[2], preferred_element_type=jnp.float32)
    summed = lax.psum((shift_part, scale_part, gate_part), "sp")
    shift_vec, scale_vec, gate_vec = (
        lax.all_gather(summed[0], "tp", axis=1, tiled=True),
        lax.all_gather(summed[1], "tp", axis=1, tiled=True),
        lax.all_gather(summed[2], "tp", axis=1, tiled=True),
    )
    key_width = w_key.shape[1]
    ctx_hidden = mod_norm(ctx_rows, norm_gain, scale_vec[1], shift_vec[1])
    own_keys = jnp.dot(ctx_hidden, w_key, preferred_element_type=jnp.float32).astype(jnp.bfloat16)
    own_values = jnp.dot(ctx_hidden, w_value, preferred_element_type=jnp.float32).astype(
        jnp.bfloat16
    )
    collected = lax.all_gather(
        jnp.concatenate([own_keys, own_values], axis=1), "sp", axis=0, tiled=True
    )
    key_ctx = collected[:, :key_width]
    value_ctx = collected[:, key_width:]
    hidden = mod_norm(latent, norm_gain, scale_vec[0], shift_vec[0])
    query = jnp.dot(hidden, w_query, preferred_element_type=jnp.float32).astype(jnp.bfloat16)
    key_rows = jnp.dot(hidden, w_key, preferred_element_type=jnp.float32).astype(jnp.bfloat16)
    value_rows = jnp.dot(hidden, w_value, preferred_element_type=jnp.float32).astype(jnp.bfloat16)
    row_count = query.shape[0]
    offset = (sp_index * tp_size + tp_index) * row_count
    seq_total = sp_size * tp_size * row_count
    cosine, sine_table = rope_angles(offset + jnp.arange(row_count, dtype=jnp.int32), head_width)
    query_heads = query.reshape(row_count, kv_count * group_size, head_width)
    query_rot = rotate(query_heads, cosine, sine_table).reshape(
        row_count, kv_count, group_size, head_width
    )
    query_grid = query_heads.reshape(row_count, kv_count, group_size, head_width)
    key_rot = rotate(key_rows.reshape(row_count, kv_count, head_width), cosine, sine_table)
    key_value = jnp.concatenate([key_rot.reshape(row_count, key_width), value_rows], axis=1)
    padded = extended(key_value, ((("sp", "tp"), 0),), SPAN)
    padded_rows = padded.shape[0]
    key_pad = padded[:, :key_width].reshape(padded_rows, kv_count, head_width)
    value_pad = padded[:, key_width:].reshape(padded_rows, kv_count, head_width)
    ctx_count = key_ctx.shape[0]

    def one_head(q_rot, q_plain, k_pad, v_pad, k_ctx, v_ctx, sink_group):
        return band_attention(
            q_rot, q_plain, k_pad, v_pad, k_ctx, v_ctx, sink_group, offset, seq_total
        )

    attended = jax.vmap(one_head, in_axes=(1, 1, 1, 1, 1, 1, 0), out_axes=1)(
        query_rot,
        query_grid,
        key_pad,
        value_pad,
        key_ctx.reshape(ctx_count, kv_count, head_width),
        value_ctx.reshape(ctx_count, kv_count, head_width),
        sink.reshape(kv_count, group_size),
    )
    mixed = attended.reshape(row_count, kv_count * group_size * head_width)
    projected = jnp.dot(mixed, w_out, preferred_element_type=jnp.float32)
    normed = (
        projected
        * lax.rsqrt(jnp.mean(projected * projected, axis=-1, keepdims=True) + EPSILON)
        * out_gain
    )
    return (latent.astype(jnp.float32) + gate_vec[0] * normed).astype(jnp.bfloat16)


def solution(mesh):
    placed = (
        P(("dp", "sp", "tp"), None),
        P("dp"),
        P(("dp", "sp"), None),
        P(),
        P(None, "sp", "tp"),
        P(),
        P(),
        P(),
        P(),
        P(),
        P(),
        P(),
    )
    return jax.shard_map(
        shards, mesh=mesh, in_specs=placed, out_specs=P(("dp", "sp", "tp"), None), check_vma=False
    )
```

profile of v0, /device:TPU:0, one launch (start us, length us, event | category | flops | bytes accessed | tf_op | source)
XLA Modules:
  0.0 130.4 jit_solution(17493451635152819227)
XLA Ops:
  6.6 0.8 stack.10
  7.4 0.7 stack.9
  8.1 1.2 fusion.27
  9.4 1.2 fusion.29
  10.6 1.2 fusion.31
  11.8 20.5 %all-reduce = (f32[2,512]{1,0:T(2,128)S(1)}, f32[2,512]{1,0:T(2,128)S(1)}, f32[1,512]{1,0:T(1,128)S(1)}) all-reduce(f32[2,512]{1,0:T(2,128)S(1)} %fusion.27, f32[2,512]{1,0:T(2,128)S(1)} %fusion.29, f32[1,512]{1,0:T(1,128)S(1)} %fusion.31), channel_id=1, replica_groups=mesh['sp'=4,'tp'=4,'dp'=2] {'sp'}, use_global_device_ids=true, to_apply=%region_3.4 | all-reduce | flops 2560 | bytes 20480 | tf_op jit(solution)/shard_map/psum | solution.py:136
  32.3 8.2 %all_gather.14 = f32[2,2048]{1,0:T(2,128)S(1)} all-gather(f32[2,512]{1,0:T(2,128)S(1)} %get-tuple-element.5), channel_id=1, replica_groups=mesh['sp'=4,'tp'=4,'dp'=2] {'tp'}, dimensions={1}, use_global_device_ids=true | all-gather | bytes 20480 | tf_op jit(solution)/shard_map/all_gather | solution.py:138
  40.5 8.2 %all_gather.13 = f32[2,2048]{1,0:T(2,128)S(1)} all-gather(f32[2,512]{1,0:T(2,128)S(1)} %get-tuple-element.6), channel_id=1, replica_groups=mesh['sp'=4,'tp'=4,'dp'=2] {'tp'}, dimensions={1}, use_global_device_ids=true | all-gather | bytes 20480 | tf_op jit(solution)/shard_map/all_gather | solution.py:139
  49.0 2.0 %convolution_convert_fusion.1 = bf16[256,256]{0,1:T(8,128)(2,1)S(1)} fusion(bf16[2048,256]{1,0:T(8,128)(2,1)} %param.21, bf16[256,2048]{1,0:T(8,128)(2,1)S(1)} %copy-done.2, f32[2048]{0:T(1024)S(1)} %bitcast.149, f32[2048]{0:T(1024)S(1)} %bitcast.151, f32[256]{0:T(256)S(1)} %add_rsqrt_fusion.1, f32[2048]{0:T(1024)S(1)} %copy-done.7), kind=kOutput, calls=%fused_computation.34 | convolution fusion | flops 271646720 | bytes 2253824 | tf_op jit(solution)/shard_map/dot_general | solution.py:145
  51.0 0.8 convolution_convert_fusion.2
  51.8 0.7 pad_maximum_fusion.1
  52.9 0.8 convolution_convert_fusion.4
  54.1 0.8 convolution_convert_fusion.3
  55.2 0.7 fusion.46
  55.9 1.3 collective-permute-start.1
  57.2 5.2 %collective-permute-start = (bf16[128,512]{0,1:T(8,128)(2,1)}, bf16[128,512]{0,1:T(8,128)(2,1)}, u32[]{:S(2)}, u32[]{:S(2)}) collective-permute-start(bf16[128,512]{0,1:T(8,128)(2,1)} %get-tuple-element.22), channel_id=1, source_target_pairs={{0,2},{2,4},{4,6},{6,8},{8,10},{10,12},{12,14},{14,16},{16,18},{18... | collective-permute-start | bytes 393224 | tf_op jit(solution)/shard_map/ppermute | solution.py:24
  62.6 4.3 %convolution_convert_fusion = bf16[256,1024]{1,0:T(8,128)(2,1)} fusion(bf16[2048,1024]{1,0:T(8,128)(2,1)} %param.19, bf16[256,2048]{1,0:T(8,128)(2,1)S(1)} %copy-done.1, f32[2048]{0:T(1024)S(1)} %bitcast.145, f32[2048]{0:T(1024)S(1)} %bitcast.148, f32[2048]{0:T(1024)S(1)} %copy-done.7, f32[256]{0:T(256)S(1)} %add_rsqrt_fusion.2), kind=kOutput, calls=%fused_computation.33 | convolution fusion | flops 1077149696 | bytes 5792768 | tf_op jit(solution)/shard_map/dot_general | solution.py:154
  66.9 1.3 copy.23
  68.1 1.0 subtract_convert_fusion
  69.2 1.2 copy.25
  70.5 7.9 %all_gather.12 = f32[1,2048]{1,0:T(1,128)S(1)} all-gather(f32[1,512]{1,0:T(1,128)S(1)} %get-tuple-element.7), channel_id=1, replica_groups=mesh['sp'=4,'tp'=4,'dp'=2] {'tp'}, dimensions={1}, use_global_device_ids=true | all-gather | bytes 10240 | tf_op jit(solution)/shard_map/all_gather | solution.py:140
  79.0 1.0 pad_maximum_fusion
  81.1 0.7 copy.40
  83.0 4.8 %fusion.4 = (f32[4,2,4,128]{3,2,1,0:T(4,128)S(1)}, f32[4,2,384,128,4]{3,2,4,1,0:T(8,128)}) fusion(pred[2,128,384]{1,2,0:T(8,128)(4,1)S(1)} %fusion.45, bf16[4,2,128,64]{2,3,1,0:T(8,128)(2,1)} %copy.41, bf16[4,2,128,64]{2,3,1,0:T(8,128)(2,1)} %copy.40, bf16[4,2,128,64]{2,3,1,0:T(8,128)(2,1)} %copy.39, bf16[256,4,4,32]{0,3,2,1:T(8,128)(2,1)} %bitcast.140, ...), kind=kOutput, calls=%fused_computation.10 | convolution fusion | flops 208269312 | bytes 7323648 | tf_op jit(solution)/shard_map/vmap(nigd,njd->ngij)/dot_general | solution.py:81
  87.8 1.3 fusion.63
  89.1 8.1 %bitcast_reduce_fusion = (f32[4,2,4,128]{3,2,1,0:T(4,128)S(1)}, f32[4,1024,2,128,4]{3,1,4,2,0:T(8,128)}) fusion(bf16[1024,4,64,1,1]{0,2,4,3,1:T(8,128)(2,1)S(1)} %bitcast.132, bf16[4,4,8,2,8,128]{5,4,3,2,1,0:T(8,128)(2,1)S(1)} %bitcast.131), kind=kOutput, calls=%fused_computation.1 | convolution fusion | flops 545255424 | bytes 17842176 | tf_op jit(solution)/shard_map/vmap(nigd,cd->ngic)/dot_general | solution.py:92
  97.3 1.4 %fusion.3 = f32[4,2,4,128]{3,2,1,0:T(4,128)S(1)} fusion(f32[4,2,384,128,4]{3,2,4,1,0:T(8,128)S(1)} %bitcast.127, f32[4,2,4,128]{3,2,1,0:T(4,128)S(1)} %maximum_maximum_fusion, pred[2,128,384]{1,2,0:T(8,128)(4,1)S(1)} %fusion.45), kind=kLoop, calls=%fused_computation.9 | loop fusion | flops 6287360 | bytes 6422528 | tf_op jit(solution)/shard_map/vmap()/reduce_sum | solution.py:100
  98.8 9.0 %fusion.1 = f32[4,2,4,128]{3,2,1,0:T(4,128)S(1)} fusion(f32[4,1024,2,128,4]{3,1,4,2,0:T(8,128)} %get-tuple-element.37, f32[4,2,4,128]{3,2,1,0:T(4,128)S(1)} %maximum_maximum_fusion), kind=kLoop, calls=%fused_computation.4 | loop fusion | flops 12578816 | bytes 16809984 | tf_op jit(solution)/shard_map/vmap()/reduce_sum | solution.py:100
  107.8 7.9 %fusion.18 = f32[4,2,128,4,64]{2,4,3,1,0:T(8,128)S(1)} fusion(bf16[1024,4,64,1,1]{0,2,4,3,1:T(8,128)(2,1)S(1)} %bitcast.138, f32[4,1024,2,128,4]{3,1,4,2,0:T(8,128)} %get-tuple-element.37, f32[4,2,4,128]{3,2,1,0:T(4,128)S(1)} %exponential_add_fusion, f32[4,2,4,128]{3,2,1,0:T(4,128)S(1)} %maximum_maximum_fusion), kind=kOutput, calls=%fused_computation.30 | convolution fusion | flops 553648128 | bytes 18382848 | tf_op jit(solution)/shard_map/vmap(ngic,cd->nigd)/dot_general | solution.py:105
  115.8 1.8 %fusion.20 = bf16[4,2,128,4,64]{2,4,3,1,0:T(8,128)(2,1)S(1)} fusion(f32[4,2,128,4,64]{2,4,3,1,0:T(8,128)S(1)} %fusion.18, f32[4,2,384,128,4]{3,2,4,1,0:T(8,128)S(1)} %bitcast.129, f32[4,2,4,128]{3,2,1,0:T(4,128)S(1)} %exponential_add_fusion, f32[4,2,4,128]{3,2,1,0:T(4,128)S(1)} %maximum_maximum_fusion, pred[2,128,384]{1,2,0:T(8,128)(4,1)S(1)} %fusion.45, ...), kind=kOutput, calls=%fused_computation.32 | convolution fusion | flops 210894848 | bytes 8388608 | tf_op jit(solution)/shard_map/vmap(ngij,njd->nigd)/dot_general | solution.py:103
  118.5 3.5 %multiply_reduce_fusion = (f32[256]{0:T(256)S(1)}, f32[256,2048]{1,0:T(8,128)S(1)}) fusion(bf16[256,1024]{0,1:T(8,128)(2,1)S(1)} %bitcast.137, bf16[1024,2048]{1,0:T(8,128)(2,1)} %param.22), kind=kOutput, calls=%fused_computation.28 | convolution fusion | flops 1074790144 | bytes 6816768 | tf_op jit(solution)/shard_map/dot_general | solution.py:189
  122.0 1.5 %fusion.16 = bf16[256,2048]{1,0:T(8,128)(2,1)} fusion(bf16[256,2048]{1,0:T(8,128)(2,1)S(1)} %copy-done.1, f32[256,2048]{1,0:T(8,128)S(1)} %get-tuple-element.39, f32[2048]{0:T(1024)S(1)} %copy-done.4, f32[256]{0:T(256)S(1)} %add_rsqrt_fusion, f32[2048]{0:T(1024)S(1)} %bitcast.142), kind=kLoop, calls=%fused_computation.27 | loop fusion | flops 3145728 | bytes 4211712 | tf_op jit(solution)/shard_map/convert_element_type | solution.py:195
  (67 shorter events, 5.5 us)
Async XLA Ops:
  6.5 44.4 %copy-start = (bf16[2048,256]{1,0:T(8,128)(2,1)S(1)}, bf16[2048,256]{1,0:T(8,128)(2,1)}, u32[]{:S(2)}) copy-start(bf16[2048,256]{1,0:T(8,128)(2,1)} %param.20) | copy-start | bytes 3145732
  6.5 42.1 %copy-start.2 = (bf16[256,2048]{1,0:T(8,128)(2,1)S(1)}, bf16[256,2048]{1,0:T(8,128)(2,1)}, u32[]{:S(2)}) copy-start(bf16[256,2048]{1,0:T(8,128)(2,1)} %param.14) | copy-start | bytes 3145732
  6.5 42.4 %copy-start.7 = (f32[2048]{0:T(1024)S(1)}, f32[2048]{0:T(1024)}, u32[]{:S(2)}) copy-start(f32[2048]{0:T(1024)} %param.17) | copy-start | bytes 24580
  6.5 81.3 %all-gather.2.cloned.1.call-start = ((), (), s32[]{:S(2)}) async-start(), calls=%async_computation | async-start | bytes 1310720 | tf_op jit(solution)/shard_map/all_gather | solution.py:148
  51.0 1.6 %copy-start.1 = (bf16[256,2048]{1,0:T(8,128)(2,1)S(1)}, bf16[256,2048]{1,0:T(8,128)(2,1)}, u32[]{:S(2)}) copy-start(bf16[256,2048]{1,0:T(8,128)(2,1)} %param.12) | copy-start | bytes 3145732
  52.8 1.2 copy-start.6
  55.9 23.0 %collective-permute-start.1 = (bf16[128,512]{0,1:T(8,128)(2,1)}, bf16[128,512]{0,1:T(8,128)(2,1)}, u32[]{:S(2)}, u32[]{:S(2)}) collective-permute-start(bf16[128,512]{0,1:T(8,128)(2,1)} %get-tuple-element.23), channel_id=1, source_target_pairs={{2,0},{4,2},{6,4},{8,6},{10,8},{12,10},{14,12},{16,14},{18,16},{20... | collective-permute-start | bytes 393224 | tf_op jit(solution)/shard_map/ppermute | solution.py:26
  57.2 21.7 %collective-permute-start = (bf16[128,512]{0,1:T(8,128)(2,1)}, bf16[128,512]{0,1:T(8,128)(2,1)}, u32[]{:S(2)}, u32[]{:S(2)}) collective-permute-start(bf16[128,512]{0,1:T(8,128)(2,1)} %get-tuple-element.22), channel_id=1, source_target_pairs={{0,2},{2,4},{4,6},{6,8},{8,10},{10,12},{12,14},{14,16},{16,18},{18... | collective-permute-start | bytes 393224 | tf_op jit(solution)/shard_map/ppermute | solution.py:24
  66.9 3.6 %copy-start.5 = (f32[16]{0:T(128)S(1)}, f32[16]{0:T(128)}, u32[]{:S(2)}) copy-start(f32[16]{0:T(128)} %param.23) | copy-start | bytes 196
  80.1 2.9 %copy-start.3 = (bf16[256,16,32]{0,2,1:T(8,128)(2,1)S(1)}, bf16[256,16,32]{0,2,1:T(8,128)(2,1)}, u32[]{:S(2)}) copy-start(bf16[256,16,32]{0,2,1:T(8,128)(2,1)} %get-tuple-element.8) | copy-start | bytes 786436
  89.1 8.2 %slice-start = ((s8[6291456]{0:T(1024)(128)(4,1)}), s8[4194304]{0:T(1024)(128)(4,1)S(1)}, s32[]{:S(2)}) async-start(s8[6291456]{0:T(1024)(128)(4,1)} %bitcast.126), calls=%async_computation.1 | async-start | bytes 8388608
  89.1 8.2 %slice-start.1 = ((s8[6291456]{0:T(1024)(128)(4,1)}), s8[2097152]{0:T(1024)(128)(4,1)S(1)}, s32[]{:S(2)}) async-start(s8[6291456]{0:T(1024)(128)(4,1)} %bitcast.126), calls=%async_computation.2 | async-start | bytes 4194304
  98.8 17.0 %slice-start.2 = ((s8[6291456]{0:T(1024)(128)(4,1)}), s8[2097152]{0:T(1024)(128)(4,1)S(1)}, s32[]{:S(2)}) async-start(s8[6291456]{0:T(1024)(128)(4,1)} %bitcast.128), calls=%async_computation.3 | async-start | bytes 4194304
  107.8 8.0 %slice-start.3 = ((s8[6291456]{0:T(1024)(128)(4,1)}), s8[4194304]{0:T(1024)(128)(4,1)S(1)}, s32[]{:S(2)}) async-start(s8[6291456]{0:T(1024)(128)(4,1)} %bitcast.128), calls=%async_computation.4 | async-start | bytes 8388608
  118.5 3.6 %copy-start.4 = (f32[2048]{0:T(1024)S(1)}, f32[2048]{0:T(1024)}, u32[]{:S(2)}) copy-start(f32[2048]{0:T(1024)} %param.18) | copy-start | bytes 24580
Sparse Core Ops, SparseCore 0:
  52.6 27.8 all-gather.1
where the time goes:
time: 131 us; the launch traced here: 130 us
  blocking collectives  44.7 us (34%)
  matrix products  38.5 us (29%)
  other arithmetic  17.2 us (13%)
  between operations  13.8 us (11%)
  local copies, waits for them, and re-layouts  9.68 us (7%)
  starting transfers between devices  6.49 us (5%)
    psum x1, blocking collectives, shards(): summed = lax.psum((shift_part, scale_part, gate_part), 'sp')  20.5 us
    reduce_sum x2, other arithmetic, band_attention(): denom = jnp.sum(exp_local, axis=-1) + jnp.sum(exp_ctx, axis=-1) + exp_sink  10.4 us
    all_gather x1, blocking collectives, shards(): lax.all_gather(summed[0], 'tp', axis=1, tiled=True)  8.18 us
    all_gather x1, blocking collectives, shards(): lax.all_gather(summed[1], 'tp', axis=1, tiled=True)  8.16 us
    dot_general x1, matrix products, band_attention(): jnp.einsum('nigd,cd->ngic', plain_blocks, key_ctx, preferred_element_type...  8.13 us
    dot_general x1, matrix products, band_attention(): jnp.einsum('ngic,cd->nigd', weight_ctx, value_ctx, preferred_element_type...  7.92 us
    all_gather x1, blocking collectives, shards(): lax.all_gather(summed[2], 'tp', axis=1, tiled=True)  7.91 us
    ppermute x1, starting transfers between devices, extended(): lax.ppermute(tail, axis, [(i, (i + 1) % count) for i in range(ends)])  5.21 us
  transfers between devices with their start and end apart: 3, of which 0 were waited for; matrix products, arithmetic and copies ran while one was open for 16% of the time, Pallas kernels for 0%

commit v1 on v0

v1 whole, which is shorter than its diff:
```python
import functools
import math

import jax
import jax.numpy as jnp
from jax import lax
from jax.experimental import pallas as pl
from jax.experimental.pallas import tpu as pltpu
from jax.sharding import PartitionSpec as P

HEAD_DIM = 64
WINDOW = 128
SPAN = 128
GRID_W = 64
EPSILON = 1e-06
NEG_BIG = -1e30
LANES = 128
MESH = pl.DeviceIdType.MESH
F32 = jnp.float32
BF16 = jnp.bfloat16


def dot(a, b):
    return jnp.dot(a, b, preferred_element_type=F32)


def dot_t(a, b):
    return lax.dot_general(a, b, (((1,), (1,)), ((), ())), preferred_element_type=F32)


def kernel(
    sp_n,
    tp_n,
    latent_hbm,
    cond_ref,
    ctx_hbm,
    ctx_cond_ref,
    mod_hbm,
    norm_gain_ref,
    out_gain_ref,
    wq_hbm,
    wk_hbm,
    wv_hbm,
    wo_hbm,
    sink_ref,
    out_ref,
    mod,
    ctx,
    wk,
    wv,
    latent,
    wq,
    wo,
    hidden,
    parts,
    vecs,
    rms,
    table,
    bias,
    ctx_kv,
    own_kv,
    q_rot,
    q_plain,
    mixed,
    projected,
    load_sem,
    sum_send,
    sum_recv,
    gat_send,
    gat_recv,
    z_send,
    z_recv,
    f_send,
    f_recv,
    halo_send,
    halo_recv,
):
    sp = lax.axis_index("sp")
    tp = lax.axis_index("tp")
    me = sp * tp_n + tp
    count = sp_n * tp_n
    rows, width = latent.shape
    ctx_rows = ctx.shape[0]
    key_width = wk.shape[1]
    kv_width = 2 * key_width
    piece = mod.shape[1]
    cols = mod.shape[2]
    quarter = ctx_rows // tp_n
    blocks = rows // SPAN
    pairs = key_width // LANES
    heads = wq.shape[1] // HEAD_DIM
    group = heads // (key_width // HEAD_DIM)

    barrier = pltpu.get_barrier_semaphore()
    for step in range(1, count):
        other = lax.rem(me + step, count)
        pl.semaphore_signal(
            barrier,
            inc=1,
            device_id={"sp": other // tp_n, "tp": lax.rem(other, tp_n)},
            device_id_type=MESH,
        )

    loads = []
    for at, (source, target) in enumerate(
        ((mod_hbm, mod), (ctx_hbm, ctx), (wk_hbm, wk), (wv_hbm, wv), (latent_hbm, latent), (wq_hbm, wq), (wo_hbm, wo))
    ):
        load = pltpu.make_async_copy(source, target, load_sem.at[at])
        load.start()
        loads.append(load)

    at_rows = pl.ds(pl.multiple_of(sp * piece, LANES), piece)
    own = []
    for ref in (cond_ref, ctx_cond_ref):
        v = ref[:, at_rows].astype(F32)
        own.append(jnp.broadcast_to(v / (1.0 + jnp.exp(-v)), (16, piece)))
    row_id = lax.broadcasted_iota(jnp.int32, (16, piece), 0)
    loads[0].wait()
    total = None
    for which in range(3):
        left = jnp.where(
            row_id == 2 * which, own[0], jnp.where(row_id == 2 * which + 1, own[1], 0.0)
        ).astype(BF16)
        term = dot(left, mod[which])
        total = term if total is None else total + term
    parts[sp] = total[:8]
    pl.semaphore_wait(barrier, count - 1)

    def sum_copy(step, slot):
        return pltpu.make_async_remote_copy(
            src_ref=parts.at[sp],
            dst_ref=parts.at[slot],
            send_sem=sum_send.at[step - 1],
            recv_sem=sum_recv.at[slot],
            device_id={"sp": lax.rem(sp + step, sp_n), "tp": tp},
            device_id_type=MESH,
        )

    for step in range(1, sp_n):
        sum_copy(step, sp).start()

    def row_rms(ref, at):
        x = ref[...].astype(F32)
        mean = jnp.sum(x * x, axis=-1, keepdims=True) * (1.0 / width)
        rms[at, : ref.shape[0]] = jnp.broadcast_to(lax.rsqrt(mean + EPSILON), (ref.shape[0], LANES))

    loads[1].wait()
    row_rms(ctx, 1)

    for step in range(1, sp_n):
        sum_copy(step, lax.rem(sp + step, sp_n)).wait_recv()
    summed = parts[0]
    for s in range(1, sp_n):
        summed = summed + parts[s]
    vecs[tp] = summed

    def gat_copy(step, slot):
        return pltpu.make_async_remote_copy(
            src_ref=vecs.at[tp],
            dst_ref=vecs.at[slot],
            send_sem=gat_send.at[step - 1],
            recv_sem=gat_recv.at[slot],
            device_id={"sp": sp, "tp": lax.rem(tp + step, tp_n)},
            device_id_type=MESH,
        )

    for step in range(1, tp_n):
        gat_copy(step, tp).start()

    loads[4].wait()
    row_rms(latent, 0)

    lane = lax.broadcasted_iota(jnp.int32, (rows, LANES), 1)
    low_half = (lane & (HEAD_DIM // 2)) == 0
    position = me * rows + lax.broadcasted_iota(jnp.int32, (rows, LANES), 0)
    freqs = HEAD_DIM // 4
    slot = (lane & (freqs - 1)).astype(F32)
    coord = jnp.where((lane & freqs) == 0, position // GRID_W, position % GRID_W).astype(F32)
    angle = coord * jnp.exp(slot * (-math.log(10000.0) / freqs))
    table[0] = jnp.cos(angle)
    sine = jnp.sin(angle)
    table[1] = jnp.where(low_half, -sine, sine)
    q_at = lax.broadcasted_iota(jnp.int32, (SPAN, 3 * SPAN), 0)
    k_at = lax.broadcasted_iota(jnp.int32, (SPAN, 3 * SPAN), 1) - SPAN
    for b in range(blocks):
        k_pos = me * rows + b * SPAN + k_at
        ok = (jnp.abs(q_at - k_at) <= WINDOW) & (k_pos >= 0) & (k_pos < count * rows)
        bias[b] = jnp.where(ok, 0.0, NEG_BIG)

    for step in range(1, tp_n):
        gat_copy(step, lax.rem(tp + step, tp_n)).wait_recv()

    def modulate(ref, which):
        r = rms[which, : ref.shape[0]]
        r = jnp.concatenate([r] * (cols // LANES), axis=1)
        for t in range(tp_n):
            at = pl.ds(t * cols, cols)
            gain = norm_gain_ref[:, at] * (1.0 + vecs[t, 2 + which : 3 + which])
            shift = vecs[t, which : which + 1]
            hidden[: ref.shape[0], at] = (ref[:, at].astype(F32) * r * gain + shift).astype(BF16)

    modulate(ctx, 1)
    loads[2].wait()
    loads[3].wait()
    ctx_at = pl.ds(pl.multiple_of(sp * ctx_rows, 16), ctx_rows)
    ctx_kv[ctx_at, :key_width] = dot(hidden[:ctx_rows], wk[...]).astype(BF16)
    ctx_kv[ctx_at, key_width:] = dot(hidden[:ctx_rows], wv[...]).astype(BF16)

    def share(s, t):
        return ctx_kv.at[pl.ds(pl.multiple_of(s * ctx_rows + t * quarter, 16), quarter)]

    def z_copy(step, s):
        return pltpu.make_async_remote_copy(
            src_ref=share(s, tp),
            dst_ref=share(s, tp),
            send_sem=z_send.at[step - 1],
            recv_sem=z_recv.at[s],
            device_id={"sp": lax.rem(sp + step, sp_n), "tp": tp},
            device_id_type=MESH,
        )

    def f_copy(far, step, s, t):
        return pltpu.make_async_remote_copy(
            src_ref=share(s, t),
            dst_ref=share(s, t),
            send_sem=f_send.at[(far - 1) * (tp_n - 1) + step - 1],
            recv_sem=f_recv.at[s * tp_n + t],
            device_id={"sp": sp, "tp": lax.rem(tp + step, tp_n)},
            device_id_type=MESH,
        )

    for step in range(1, sp_n):
        z_copy(step, sp).start()

    def rotate(x):
        swapped = jnp.where(
            low_half, pltpu.roll(x, LANES - HEAD_DIM // 2, 1), pltpu.roll(x, HEAD_DIM // 2, 1)
        )
        return x * table[0] + swapped * table[1]

    modulate(latent, 0)
    keys = dot(hidden[:rows], wk[...]).astype(BF16).astype(F32)
    for p in range(pairs):
        at = slice(p * LANES, (p + 1) * LANES)
        own_kv[SPAN : SPAN + rows, at] = rotate(keys[:, at]).astype(BF16)
    own_kv[SPAN : SPAN + rows, key_width:] = dot(hidden[:rows], wv[...]).astype(BF16)

    after = lax.rem(me + 1, count)
    before = lax.rem(me + count - 1, count)
    to_next = pltpu.make_async_remote_copy(
        src_ref=own_kv.at[pl.ds(rows, SPAN)],
        dst_ref=own_kv.at[pl.ds(0, SPAN)],
        send_sem=halo_send.at[0],
        recv_sem=halo_recv.at[0],
        device_id={"sp": after // tp_n, "tp": lax.rem(after, tp_n)},
        device_id_type=MESH,
    )
    to_prev = pltpu.make_async_remote_copy(
        src_ref=own_kv.at[pl.ds(SPAN, SPAN)],
        dst_ref=own_kv.at[pl.ds(SPAN + rows, SPAN)],
        send_sem=halo_send.at[1],
        recv_sem=halo_recv.at[1],
        device_id={"sp": before // tp_n, "tp": lax.rem(before, tp_n)},
        device_id_type=MESH,
    )

    @pl.when(me < count - 1)
    def _():
        to_next.start()

    @pl.when(me > 0)
    def _():
        to_prev.start()

    @pl.when(me == 0)
    def _():
        own_kv[:SPAN] = jnp.zeros((SPAN, kv_width), BF16)

    @pl.when(me == count - 1)
    def _():
        own_kv[SPAN + rows :] = jnp.zeros((SPAN, kv_width), BF16)

    in_low = lane < HEAD_DIM
    loads[5].wait()
    tile = group * HEAD_DIM
    for kv in range(heads // group):
        q = dot(hidden[:rows], wq[:, kv * tile : (kv + 1) * tile]).astype(BF16).astype(F32)
        q = q * (HEAD_DIM**-0.5)
        keep = in_low if kv % 2 == 0 else jnp.logical_not(in_low)
        for j in range(tile // LANES):
            plain = q[:, j * LANES : (j + 1) * LANES]
            for target, x in ((q_plain, plain), (q_rot, rotate(plain))):
                turned = pltpu.roll(x, HEAD_DIM, 1)
                first, second = (x, turned) if kv % 2 == 0 else (turned, x)
                h = kv * group + 2 * j
                target[h] = jnp.where(keep, first, 0.0).astype(BF16)
                target[h + 1] = jnp.where(keep, second, 0.0).astype(BF16)

    for far in range(1, sp_n):
        s = lax.rem(sp + sp_n - far, sp_n)
        z_copy(far, s).wait_recv()
        for step in range(1, tp_n):
            f_copy(far, step, s, tp).start()

    @pl.when(me > 0)
    def _():
        to_next.wait_recv()

    @pl.when(me < count - 1)
    def _():
        to_prev.wait_recv()

    for far in range(1, sp_n):
        s = lax.rem(sp + sp_n - far, sp_n)
        for step in range(1, tp_n):
            f_copy(far, step, s, lax.rem(tp + step, tp_n)).wait_recv()

    half_tiles = tile // LANES

    def attend(at, carry):
        pair = at // half_tiles
        half = lax.rem(at, half_tiles)
        k_lanes = pl.ds(pl.multiple_of(pair * LANES, LANES), LANES)
        v_lanes = pl.ds(pl.multiple_of(key_width + pair * LANES, LANES), LANES)
        k_ctx = ctx_kv[:, k_lanes]
        v_ctx = ctx_kv[:, v_lanes]
        v_ctx = jnp.concatenate([v_ctx, jnp.ones(v_ctx.shape, BF16)], axis=1)
        for parity in range(2):
            out = []
            lane_tile = (pair * 2 + parity) * half_tiles + half
            for a in range(2):
                h = lane_tile * 2 + a
                s_ctx = dot_t(q_plain[h], k_ctx)
                tops, locals_ = [], []
                for b in range(blocks):
                    s_loc = (
                        dot_t(
                            q_rot[h, b * SPAN : (b + 1) * SPAN],
                            own_kv[b * SPAN : (b + 3) * SPAN, k_lanes],
                        )
                        + bias[b]
                    )
                    locals_.append(s_loc)
                    tops.append(jnp.max(s_loc, axis=-1, keepdims=True))
                sink = sink_ref[h]
                top = jnp.maximum(
                    jnp.maximum(
                        jnp.concatenate(tops, axis=0), jnp.max(s_ctx, axis=-1, keepdims=True)
                    ),
                    sink,
                )
                acc = dot(jnp.exp(s_ctx - top).astype(BF16), v_ctx)
                near = []
                for b in range(blocks):
                    v_loc = own_kv[b * SPAN : (b + 3) * SPAN, v_lanes]
                    v_loc = jnp.concatenate([v_loc, jnp.ones(v_loc.shape, BF16)], axis=1)
                    w = jnp.exp(locals_[b] - top[b * SPAN : (b + 1) * SPAN]).astype(BF16)
                    near.append(dot(w, v_loc))
                acc = acc + jnp.concatenate(near, axis=0)
                out.append(acc[:, :LANES] / (acc[:, LANES:] + jnp.exp(sink - top)))
            if parity == 0:
                both = jnp.where(in_low, out[0], pltpu.roll(out[1], HEAD_DIM, 1))
            else:
                both = jnp.where(in_low, pltpu.roll(out[0], HEAD_DIM, 1), out[1])
            mixed[:, pl.ds(pl.multiple_of(lane_tile * LANES, LANES), LANES)] = both.astype(BF16)
        return carry

    lax.fori_loop(0, pairs * half_tiles, attend, 0)

    loads[6].wait()
    wide = 256

    def project(at, squares):
        lanes = pl.ds(pl.multiple_of(at * wide, wide), wide)
        y = dot(mixed[...], wo[:, lanes])
        projected[:, lanes] = y
        return squares + jnp.sum(y * y, axis=-1, keepdims=True)

    squares = lax.fori_loop(0, width // wide, project, jnp.zeros((rows, 1), F32))
    r = lax.rsqrt(squares * (1.0 / width) + EPSILON)
    for t in range(tp_n):
        at = pl.ds(t * cols, cols)
        gain = vecs[t, 4:5] * out_gain_ref[:, at]
        out_ref[:, at] = (latent[:, at].astype(F32) + projected[:, at] * r * gain).astype(BF16)

    for step in range(1, sp_n):
        sum_copy(step, sp).wait_send()
        z_copy(step, sp).wait_send()
    for step in range(1, tp_n):
        gat_copy(step, tp).wait_send()
        for far in range(1, sp_n):
            s = lax.rem(sp + sp_n - far, sp_n)
            f_copy(far, step, s, tp).wait_send()

    @pl.when(me < count - 1)
    def _():
        to_next.wait_send()

    @pl.when(me > 0)
    def _():
        to_prev.wait_send()


def solution(mesh):
    sp_n, tp_n = mesh.shape["sp"], mesh.shape["tp"]

    def shards(
        latent, cond, ctx_rows, ctx_cond, mod_weight, norm_gain, out_gain, w_query, w_key, w_value, w_out, sink
    ):
        rows, width = latent.shape
        context = ctx_rows.shape[0]
        key_width = w_key.shape[1]
        heads = w_query.shape[1] // HEAD_DIM
        cols = mod_weight.shape[2]
        any_spec = pl.BlockSpec(memory_space=pl.ANY)
        vmem = pl.BlockSpec(memory_space=pltpu.VMEM)
        dma = pltpu.SemaphoreType.DMA
        return pl.pallas_call(
            functools.partial(kernel, sp_n, tp_n),
            out_shape=jax.ShapeDtypeStruct((rows, width), BF16),
            in_specs=[
                any_spec,
                vmem,
                any_spec,
                vmem,
                any_spec,
                vmem,
                vmem,
                any_spec,
                any_spec,
                any_spec,
                any_spec,
                pl.BlockSpec(memory_space=pltpu.SMEM),
            ],
            out_specs=vmem,
            scratch_shapes=[
                pltpu.VMEM(mod_weight.shape, BF16),
                pltpu.VMEM(ctx_rows.shape, BF16),
                pltpu.VMEM(w_key.shape, BF16),
                pltpu.VMEM(w_value.shape, BF16),
                pltpu.VMEM(latent.shape, BF16),
                pltpu.VMEM(w_query.shape, BF16),
                pltpu.VMEM(w_out.shape, BF16),
                pltpu.VMEM((max(rows, context), width), BF16),
                pltpu.VMEM((sp_n, 8, cols), F32),
                pltpu.VMEM((tp_n, 8, cols), F32),
                pltpu.VMEM((2, max(rows, context), LANES), F32),
                pltpu.VMEM((2, rows, LANES), F32),
                pltpu.VMEM((rows // SPAN, SPAN, 3 * SPAN), F32),
                pltpu.VMEM((sp_n * context, 2 * key_width), BF16),
                pltpu.VMEM((rows + 2 * SPAN, 2 * key_width), BF16),
                pltpu.VMEM((heads, rows, LANES), BF16),
                pltpu.VMEM((heads, rows, LANES), BF16),
                pltpu.VMEM((rows, heads * HEAD_DIM), BF16),
                pltpu.VMEM((rows, width), F32),
                dma((7,)),
                dma((sp_n - 1,)),
                dma((sp_n,)),
                dma((tp_n - 1,)),
                dma((tp_n,)),
                dma((sp_n - 1,)),
                dma((sp_n,)),
                dma(((sp_n - 1) * (tp_n - 1),)),
                dma((sp_n * tp_n,)),
                dma((2,)),
                dma((2,)),
            ],
            compiler_params=pltpu.CompilerParams(
                collective_id=0, has_side_effects=True, vmem_limit_bytes=60 * 1024 * 1024
            ),
        )(
            latent,
            cond.reshape(1, -1),
            ctx_rows,
            ctx_cond.reshape(1, -1),
            mod_weight,
            norm_gain.reshape(1, -1),
            out_gain.reshape(1, -1),
            w_query,
            w_key,
            w_value,
            w_out,
            sink,
        )

    placed = (
        P(("dp", "sp", "tp"), None),
        P("dp"),
        P(("dp", "sp"), None),
        P(),
        P(None, "sp", "tp"),
        P(),
        P(),
        P(),
        P(),
        P(),
        P(),
        P(),
    )
    return jax.shard_map(
        shards, mesh=mesh, in_specs=placed, out_specs=P(("dp", "sp", "tp"), None), check_vma=False
    )
```

time: 131 us -> 52.9 us (0.40)
  Pallas kernels: 0 us -> 47.8 us
  blocking collectives: 44.7 us -> 0 us
  matrix products: 38.5 us -> 0 us
  other arithmetic: 17.2 us -> 0 us
  between operations: 13.8 us -> 0.01 us
  starting transfers between devices: 6.49 us -> 0 us
  local copies, waits for them, and re-layouts: 9.68 us -> 4.88 us
    pallas_call x0 -> x1, Pallas kernels: none -> 47.8 us  [shards(): pl.pallas_call(functools.partial(kernel, sp_n, tp_n), out_shape=jax.Shape...]
    dot_general x13 -> x0, matrix products: 38.5 us -> none  [the longest x1 8.13 us: band_attention(): jnp.einsum('nigd,cd->ngic', plain_blocks, key_ctx, preferred_element_type...]
    all_gather x3 -> x0, blocking collectives: 24.3 us -> none  [the longest x1 8.18 us: shards(): lax.all_gather(summed[0], 'tp', axis=1, tiled=True)]
    psum x1 -> x0, blocking collectives: 20.5 us -> none  [shards(): summed = lax.psum((shift_part, scale_part, gate_part), 'sp')]
    reduce_sum x4 -> x0, other arithmetic: 11 us -> none  [the longest x2 10.4 us: band_attention(): denom = jnp.sum(exp_local, axis=-1) + jnp.sum(exp_ctx, axis=-1) + exp_sink]
    ppermute x2 -> x0, starting transfers between devices: 6.49 us -> none  [the longest x1 5.21 us: extended(): lax.ppermute(tail, axis, [(i, (i + 1) % count) for i in range(ends)])]
    convert_element_type x3 -> x0, local copies, waits for them, and re-layouts: 3.05 us -> none  [the longest x1 1.26 us: rotate(): floats = values.astype(jnp.float32)]
    concatenate x4 -> x0, other arithmetic: 2.53 us -> none  [the longest x1 1.03 us: extended(): jnp.concatenate([lax.ppermute(tail, axis, [(i, (i + 1) % count) for i in...]
  transfers between devices with their start and end apart: 3 -> 0, of which waited for: 0 -> 0; matrix products, arithmetic and copies ran while one was open for 16% -> 0% of each run, Pallas kernels for 0% -> 0%
where the time goes in v1:
time: 52.9 us; the launch traced here: 52.7 us
  Pallas kernels  47.8 us (90%)
  local copies, waits for them, and re-layouts  4.88 us (9%)
    pallas_call x1, Pallas kernels, shards(): pl.pallas_call(functools.partial(kernel, sp_n, tp_n), out_shape=jax.Shape...  47.8 us
    unnamed x1, local copies, waits for them, and re-layouts  2.3 us
    reshape x1, local copies, waits for them, and re-layouts, shards(): cond.reshape(1, -1)  1.29 us
    reshape x1, local copies, waits for them, and re-layouts, shards(): ctx_cond.reshape(1, -1)  1.28 us

profile of v1, /device:TPU:0, one launch (start us, length us, event | category | flops | bytes accessed | tf_op | source)
XLA Modules:
  0.0 52.7 jit_solution(7887219867486304310)
XLA Ops:
  0.0 1.3 %reshape.12.cond_ref = bf16[1,2048]{1,0:T(2,128)(2,1)} reshape(bf16[2048]{0:T(1024)(128)(2,1)} %param.13) | data formatting | bytes 8192 | tf_op jit(solution)/shard_map/reshape | solution.py:473
  1.3 1.3 %reshape.13.ctx_cond_ref = bf16[1,2048]{1,0:T(2,128)(2,1)} reshape(bf16[2048]{0:T(1024)(128)(2,1)} %param.15) | data formatting | bytes 8192 | tf_op jit(solution)/shard_map/reshape | solution.py:475
  2.6 47.8 %shard_map.118 = bf16[256,2048]{1,0:T(8,128)(2,1)} custom-call(bf16[256,2048]{1,0:T(8,128)(2,1)} %latent_hbm.1, bf16[1,2048]{1,0:T(2,128)(2,1)} %reshape.12.cond_ref, bf16[256,2048]{1,0:T(8,128)(2,1)} %ctx_hbm.1, bf16[1,2048]{1,0:T(2,128)(2,1)} %reshape.13.ctx_cond_ref, bf16[3,512,512]{2,1,0:T(8,128)(2,1)} %mod_hbm.1, f32[1,2048]{1,0:T(1,128)} %bitcast.2, ...), custom_call_target="tpu_custom_call" | custom-call | tf_op jit(solution)/shard_map/pallas_call | solution.py:418
  50.3 2.3 %copy.14 = bf16[256,2048]{1,0:T(8,128)(2,1)} copy(bf16[256,2048]{1,0:T(8,128)(2,1)} %shard_map.118) | data formatting | bytes 2097152

commit v2 on v1

--- a/solution.py
+++ b/solution.py
@@ -52,6 +52,7 @@
     wq,
     wo,
     hidden,
+    silu,
     parts,
     vecs,
     rms,
@@ -61,6 +62,8 @@
     own_kv,
     q_rot,
     q_plain,
+    acc,
+    tops,
     mixed,
     projected,
     load_sem,
@@ -78,6 +81,7 @@
     sp = lax.axis_index("sp")
     tp = lax.axis_index("tp")
     me = sp * tp_n + tp
+    way = 1 - 2 * ((2 * sp) // sp_n)
     count = sp_n * tp_n
     rows, width = latent.shape
     ctx_rows = ctx.shape[0]
@@ -109,11 +113,14 @@
         load.start()
         loads.append(load)
 
-    at_rows = pl.ds(pl.multiple_of(sp * piece, LANES), piece)
     own = []
-    for ref in (cond_ref, ctx_cond_ref):
-        v = ref[:, at_rows].astype(F32)
-        own.append(jnp.broadcast_to(v / (1.0 + jnp.exp(-v)), (16, piece)))
+    for which, ref in enumerate((cond_ref, ctx_cond_ref)):
+        v = ref[...].astype(F32)
+        silu[which] = v / (1.0 + jnp.exp(-v))
+        tiles = [
+            silu[which, pl.ds(sp * (piece // LANES) + i, 1)] for i in range(piece // LANES)
+        ]
+        own.append(jnp.broadcast_to(jnp.concatenate(tiles, axis=1), (16, piece)))
     row_id = lax.broadcasted_iota(jnp.int32, (16, piece), 0)
     loads[0].wait()
     total = None
@@ -206,6 +213,9 @@
     ctx_kv[ctx_at, :key_width] = dot(hidden[:ctx_rows], wk[...]).astype(BF16)
     ctx_kv[ctx_at, key_width:] = dot(hidden[:ctx_rows], wv[...]).astype(BF16)
 
+    def peer(step):
+        return lax.rem(sp + way * step + sp_n, sp_n)
+
     def share(s, t):
         return ctx_kv.at[pl.ds(pl.multiple_of(s * ctx_rows + t * quarter, 16), quarter)]
 
@@ -215,7 +225,7 @@
             dst_ref=share(s, tp),
             send_sem=z_send.at[step - 1],
             recv_sem=z_recv.at[s],
-            device_id={"sp": lax.rem(sp + step, sp_n), "tp": tp},
+            device_id={"sp": peer(step), "tp": tp},
             device_id_type=MESH,
         )
 
@@ -296,12 +306,56 @@
                 target[h] = jnp.where(keep, first, 0.0).astype(BF16)
                 target[h + 1] = jnp.where(keep, second, 0.0).astype(BF16)
 
-    for far in range(1, sp_n):
-        s = lax.rem(sp + sp_n - far, sp_n)
+    kv_heads = heads // group
+    per = -(-(sp_n - 1) // kv_heads)
+
+    def lanes_of(kv):
+        pair = kv // 2
+        return (
+            pl.ds(pl.multiple_of(pair * LANES, LANES), LANES),
+            pl.ds(pl.multiple_of(key_width + pair * LANES, LANES), LANES),
+        )
+
+    def with_ones(v):
+        return jnp.concatenate([v, jnp.ones(v.shape, BF16)], axis=1)
+
+    def forward(far):
+        s = peer(far)
         z_copy(far, s).wait_recv()
         for step in range(1, tp_n):
             f_copy(far, step, s, tp).start()
 
+    def own_block(kv, carry):
+        for i in range(per):
+            far = kv * per + i + 1
+
+            @pl.when(far < sp_n)
+            def _():
+                forward(far)
+
+        k_lanes, v_lanes = lanes_of(kv)
+        k = ctx_kv[ctx_at, k_lanes]
+        v = with_ones(ctx_kv[ctx_at, v_lanes])
+        for g in range(group):
+            h = kv * group + g
+            scores = dot_t(q_plain[h], k)
+            sink = sink_ref[h]
+            top = jnp.maximum(jnp.max(scores, axis=-1, keepdims=True), sink)
+            weights = jnp.exp(scores - top).astype(BF16)
+            term = dot(weights, v)
+            acc[h, :, :LANES] = term[:, :LANES]
+            acc[h, :, LANES:] = term[:, LANES:] + jnp.exp(sink - top)
+            tops[h] = jnp.broadcast_to(top, (rows, LANES))
+        return carry
+
+    lax.fori_loop(0, kv_heads, own_block, 0)
+
+    def update(h, at, old, top, term):
+        decay = jnp.exp(old - top)
+        acc[h, at, :LANES] = acc[h, at, :LANES] * decay + term[:, :LANES]
+        acc[h, at, LANES:] = acc[h, at, LANES:] * decay + term[:, LANES:]
+        tops[h, at] = top
+
     @pl.when(me > 0)
     def _():
         to_next.wait_recv()
@@ -310,62 +364,57 @@
     def _():
         to_prev.wait_recv()
 
-    for far in range(1, sp_n):
-        s = lax.rem(sp + sp_n - far, sp_n)
+    def window(kv, carry):
+        k_lanes, v_lanes = lanes_of(kv)
+        for b in range(blocks):
+            at = pl.ds(b * SPAN, SPAN)
+            band = pl.ds(b * SPAN, 3 * SPAN)
+            k = own_kv[band, k_lanes]
+            v = with_ones(own_kv[band, v_lanes])
+            for g in range(group):
+                h = kv * group + g
+                scores = dot_t(q_rot[h, at], k) + bias[b]
+                old = tops[h, at]
+                top = jnp.maximum(old, jnp.max(scores, axis=-1, keepdims=True))
+                weights = jnp.exp(scores - jnp.concatenate([top] * 3, axis=1)).astype(BF16)
+                update(h, at, old, top, dot(weights, v))
+        return carry
+
+    lax.fori_loop(0, kv_heads, window, 0)
+
+    def far_block(far, carry):
+        s = peer(far)
         for step in range(1, tp_n):
             f_copy(far, step, s, lax.rem(tp + step, tp_n)).wait_recv()
+        block = pl.ds(pl.multiple_of(s * ctx_rows, 16), ctx_rows)
+
+        def one(kv, inner):
+            k_lanes, v_lanes = lanes_of(kv)
+            k = ctx_kv[block, k_lanes]
+            v = with_ones(ctx_kv[block, v_lanes])
+            for g in range(group):
+                h = kv * group + g
+                scores = dot_t(q_plain[h], k)
+                old = tops[h]
+                top = jnp.maximum(old, jnp.max(scores, axis=-1, keepdims=True))
+                weights = jnp.exp(scores - top[:, :1]).astype(BF16)
+                update(h, pl.ds(0, rows), old, top, dot(weights, v))
+            return inner
+
+        return lax.fori_loop(0, kv_heads, one, carry)
+
+    lax.fori_loop(1, sp_n, far_block, 0)
 
     half_tiles = tile // LANES
-
-    def attend(at, carry):
-        pair = at // half_tiles
-        half = lax.rem(at, half_tiles)
-        k_lanes = pl.ds(pl.multiple_of(pair * LANES, LANES), LANES)
-        v_lanes = pl.ds(pl.multiple_of(key_width + pair * LANES, LANES), LANES)
-        k_ctx = ctx_kv[:, k_lanes]
-        v_ctx = ctx_kv[:, v_lanes]
-        v_ctx = jnp.concatenate([v_ctx, jnp.ones(v_ctx.shape, BF16)], axis=1)
-        for parity in range(2):
-            out = []
-            lane_tile = (pair * 2 + parity) * half_tiles + half
-            for a in range(2):
-                h = lane_tile * 2 + a
-                s_ctx = dot_t(q_plain[h], k_ctx)
-                tops, locals_ = [], []
-                for b in range(blocks):
-                    s_loc = (
-                        dot_t(
-                            q_rot[h, b * SPAN : (b + 1) * SPAN],
-                            own_kv[b * SPAN : (b + 3) * SPAN, k_lanes],
-                        )
-                        + bias[b]
-                    )
-                    locals_.append(s_loc)
-                    tops.append(jnp.max(s_loc, axis=-1, keepdims=True))
-                sink = sink_ref[h]
-                top = jnp.maximum(
-                    jnp.maximum(
-                        jnp.concatenate(tops, axis=0), jnp.max(s_ctx, axis=-1, keepdims=True)
-                    ),
-                    sink,
-                )
-                acc = dot(jnp.exp(s_ctx - top).astype(BF16), v_ctx)
-                near = []
-                for b in range(blocks):
-                    v_loc = own_kv[b * SPAN : (b + 3) * SPAN, v_lanes]
-                    v_loc = jnp.concatenate([v_loc, jnp.ones(v_loc.shape, BF16)], axis=1)
-                    w = jnp.exp(locals_[b] - top[b * SPAN : (b + 1) * SPAN]).astype(BF16)
-                    near.append(dot(w, v_loc))
-                acc = acc + jnp.concatenate(near, axis=0)
-                out.append(acc[:, :LANES] / (acc[:, LANES:] + jnp.exp(sink - top)))
-            if parity == 0:
-                both = jnp.where(in_low, out[0], pltpu.roll(out[1], HEAD_DIM, 1))
-            else:
-                both = jnp.where(in_low, pltpu.roll(out[0], HEAD_DIM, 1), out[1])
-            mixed[:, pl.ds(pl.multiple_of(lane_tile * LANES, LANES), LANES)] = both.astype(BF16)
-        return carry
-
-    lax.fori_loop(0, pairs * half_tiles, attend, 0)
+    for lane_tile in range(heads // 2):
+        out = []
+        for h in (2 * lane_tile, 2 * lane_tile + 1):
+            out.append(acc[h, :, :LANES] / acc[h, :, LANES:])
+        if (lane_tile // half_tiles) % 2 == 0:
+            both = jnp.where(in_low, out[0], pltpu.roll(out[1], HEAD_DIM, 1))
+        else:
+            both = jnp.where(in_low, pltpu.roll(out[0], HEAD_DIM, 1), out[1])
+        mixed[:, lane_tile * LANES : (lane_tile + 1) * LANES] = both.astype(BF16)
 
     loads[6].wait()
     wide = 256
@@ -389,7 +438,7 @@
     for step in range(1, tp_n):
         gat_copy(step, tp).wait_send()
         for far in range(1, sp_n):
-            s = lax.rem(sp + sp_n - far, sp_n)
+            s = peer(far)
             f_copy(far, step, s, tp).wait_send()
 
     @pl.when(me < count - 1)
@@ -442,6 +491,7 @@
                 pltpu.VMEM(w_query.shape, BF16),
                 pltpu.VMEM(w_out.shape, BF16),
                 pltpu.VMEM((max(rows, context), width), BF16),
+                pltpu.VMEM((2, width // LANES, LANES), F32),
                 pltpu.VMEM((sp_n, 8, cols), F32),
                 pltpu.VMEM((tp_n, 8, cols), F32),
                 pltpu.VMEM((2, max(rows, context), LANES), F32),
@@ -451,6 +501,8 @@
                 pltpu.VMEM((rows + 2 * SPAN, 2 * key_width), BF16),
                 pltpu.VMEM((heads, rows, LANES), BF16),
                 pltpu.VMEM((heads, rows, LANES), BF16),
+                pltpu.VMEM((heads, rows, 2 * LANES), F32),
+                pltpu.VMEM((heads, rows, LANES), F32),
                 pltpu.VMEM((rows, heads * HEAD_DIM), BF16),
                 pltpu.VMEM((rows, width), F32),
                 dma((7,)),
@@ -470,9 +522,9 @@
             ),
         )(
             latent,
-            cond.reshape(1, -1),
+            cond.reshape(-1, LANES),
             ctx_rows,
-            ctx_cond.reshape(1, -1),
+            ctx_cond.reshape(-1, LANES),
             mod_weight,
             norm_gain.reshape(1, -1),
             out_gain.reshape(1, -1),

time: 52.9 us -> 46.4 us (0.88)
  Pallas kernels: 47.8 us -> 43.9 us
  local copies, waits for them, and re-layouts: 4.88 us -> 2.3 us
    pallas_call x1, Pallas kernels: 47.8 us -> 43.9 us  [shards(): pl.pallas_call(functools.partial(kernel, sp_n, tp_n), out_shape=jax.Shape...]
    reshape x2 -> x0, local copies, waits for them, and re-layouts: 2.57 us -> none  [the longest x1 1.29 us: shards(): cond.reshape(1, -1)]
where the time goes in v2:
time: 46.4 us; the launch traced here: 46.2 us
  Pallas kernels  43.9 us (95%)
  local copies, waits for them, and re-layouts  2.3 us (5%)
    pallas_call x1, Pallas kernels, shards(): pl.pallas_call(functools.partial(kernel, sp_n, tp_n), out_shape=jax.Shape...  43.9 us
    unnamed x1, local copies, waits for them, and re-layouts  2.3 us

profile of v2, /device:TPU:0, one launch (start us, length us, event | category | flops | bytes accessed | tf_op | source)
XLA Modules:
  0.0 46.2 jit_solution(9363339375888113130)
XLA Ops:
  0.0 43.9 %shard_map.118 = bf16[256,2048]{1,0:T(8,128)(2,1)} custom-call(bf16[256,2048]{1,0:T(8,128)(2,1)} %latent_hbm.1, bf16[16,128]{1,0:T(8,128)(2,1)} %bitcast.6, bf16[256,2048]{1,0:T(8,128)(2,1)} %ctx_hbm.1, bf16[16,128]{1,0:T(8,128)(2,1)} %bitcast.7, bf16[3,512,512]{2,1,0:T(8,128)(2,1)} %mod_hbm.1, f32[1,2048]{1,0:T(1,128)} %bitcast.4, f32[1,2048]{1,0:T(1,128)} %bitcast.5, ...), custom_call_target="tpu_custom_call" | custom-call | tf_op jit(solution)/shard_map/pallas_call | solution.py:467
  43.9 2.3 %copy.14 = bf16[256,2048]{1,0:T(8,128)(2,1)} copy(bf16[256,2048]{1,0:T(8,128)(2,1)} %shard_map.118) | data formatting | bytes 2097152

commit v3 on v2

--- a/solution.py
+++ b/solution.py
@@ -95,6 +95,13 @@
     heads = wq.shape[1] // HEAD_DIM
     group = heads // (key_width // HEAD_DIM)
 
+    loads = []
+    for at, (source, target) in enumerate(
+        ((mod_hbm, mod), (ctx_hbm, ctx), (wk_hbm, wk), (wv_hbm, wv), (latent_hbm, latent), (wq_hbm, wq), (wo_hbm, wo))
+    ):
+        loads.append(pltpu.make_async_copy(source, target, load_sem.at[at]))
+    loads[0].start()
+
     barrier = pltpu.get_barrier_semaphore()
     for step in range(1, count):
         other = lax.rem(me + step, count)
@@ -104,14 +111,6 @@
             device_id={"sp": other // tp_n, "tp": lax.rem(other, tp_n)},
             device_id_type=MESH,
         )
-
-    loads = []
-    for at, (source, target) in enumerate(
-        ((mod_hbm, mod), (ctx_hbm, ctx), (wk_hbm, wk), (wv_hbm, wv), (latent_hbm, latent), (wq_hbm, wq), (wo_hbm, wo))
-    ):
-        load = pltpu.make_async_copy(source, target, load_sem.at[at])
-        load.start()
-        loads.append(load)
 
     own = []
     for which, ref in enumerate((cond_ref, ctx_cond_ref)):
@@ -123,6 +122,8 @@
         own.append(jnp.broadcast_to(jnp.concatenate(tiles, axis=1), (16, piece)))
     row_id = lax.broadcasted_iota(jnp.int32, (16, piece), 0)
     loads[0].wait()
+    for at in (1, 2, 3, 4):
+        loads[at].start()
     total = None
     for which in range(3):
         left = jnp.where(
@@ -152,6 +153,7 @@
         rms[at, : ref.shape[0]] = jnp.broadcast_to(lax.rsqrt(mean + EPSILON), (ref.shape[0], LANES))
 
     loads[1].wait()
+    loads[5].start()
     row_rms(ctx, 1)
 
     for step in range(1, sp_n):
@@ -176,6 +178,7 @@
 
     loads[4].wait()
     row_rms(latent, 0)
+    loads[6].start()
 
     lane = lax.broadcasted_iota(jnp.int32, (rows, LANES), 1)
     low_half = (lane & (HEAD_DIM // 2)) == 0

time: 46.4 us -> 46.4 us (level)
  no operation moved by 1% of the time
where the time goes in v3:
time: 46.4 us; the launch traced here: 46.2 us
  Pallas kernels  43.9 us (95%)
  local copies, waits for them, and re-layouts  2.3 us (5%)
    pallas_call x1, Pallas kernels, shards(): pl.pallas_call(functools.partial(kernel, sp_n, tp_n), out_shape=jax.Shape...  43.9 us
    unnamed x1, local copies, waits for them, and re-layouts  2.3 us

profile of v3, /device:TPU:0, one launch (start us, length us, event | category | flops | bytes accessed | tf_op | source)
XLA Modules:
  0.0 46.2 jit_solution(10338906578778643682)
XLA Ops:
  0.0 43.9 %shard_map.118 = bf16[256,2048]{1,0:T(8,128)(2,1)} custom-call(bf16[256,2048]{1,0:T(8,128)(2,1)} %latent_hbm.1, bf16[16,128]{1,0:T(8,128)(2,1)} %bitcast.6, bf16[256,2048]{1,0:T(8,128)(2,1)} %ctx_hbm.1, bf16[16,128]{1,0:T(8,128)(2,1)} %bitcast.7, bf16[3,512,512]{2,1,0:T(8,128)(2,1)} %mod_hbm.1, f32[1,2048]{1,0:T(1,128)} %bitcast.4, f32[1,2048]{1,0:T(1,128)} %bitcast.5, ...), custom_call_target="tpu_custom_call" | custom-call | tf_op jit(solution)/shard_map/pallas_call | solution.py:470
  43.9 2.3 %copy.14 = bf16[256,2048]{1,0:T(8,128)(2,1)} copy(bf16[256,2048]{1,0:T(8,128)(2,1)} %shard_map.118) | data formatting | bytes 2097152
